TPU v7x, 32 devices: a whole 2x2x4 slice. The times are simulated.
32 devices in a mesh: sp: 8 (over z, core), tp: 4 (over y, x).
Axes of the slice: x: 2, y: 2, z: 4, core: 2. Of those that a mesh axis runs over, the one named last changes fastest.
Arguments:
- residual: bfloat16 [1024, 4096], P('sp', 'tp'), may hold values from -46 to 46
- query_small: bfloat16 [1024, 2048], P('sp', 'tp'), may hold values from -6 to 6
- key_narrow_group: bfloat16 [1024, 2048], P('sp', 'tp'), may hold values from -6 to 6
- query_large: bfloat16 [1024, 4096], P('sp', 'tp'), may hold values from -6 to 6
- key_large: bfloat16 [1024, 4096], P('sp', 'tp'), may hold values from -6 to 6
- values: bfloat16 [1024, 2, 2048], P('sp', None, 'tp'), may hold values from -6 to 6
- gates: bfloat16 [1024, 2, 2048], P('sp', None, 'tp'), may hold values from -6 to 6
- log_decay: float32 [1024, 2, 16], P('sp', None, 'tp'), may hold values from -0.65 to 0, as said below
- head_gain: float32 [2, 2048], P(None, 'tp'), may hold values from 0.1 to 1.9
- out_weight: bfloat16 [2, 2048, 4096], P(None, 'sp', 'tp'), may hold values from -0.09375 to 0.09375
- norm_gain: float32 [4096], P('tp'), may hold values from 0.1 to 1.9
- routes: int32 [1024, 2], P('sp'), may hold values from 0 to 7, all different within a row; in each aligned block of 128 rows (0 to 127, 128 to 255, ...) at most 64 rows name the same one
- route_weight: float32 [1024, 2], P('sp'), may hold values from 0.2 to 1
- expert_gate: bfloat16 [8, 4096, 2048], P('sp', None, 'tp'), may hold values from -0.09375 to 0.09375
- expert_up: bfloat16 [8, 4096, 2048], P('sp', None, 'tp'), may hold values from -0.09375 to 0.09375
- expert_down: bfloat16 [8, 2048, 4096], P('sp', None, 'tp'), may hold values from -0.5 to 0.5
Outputs:
- new_stream: bfloat16 [1024, 4096], P('sp', 'tp')
Inputs may be any that keep to these rules, and one draw needn't show every extreme that they name: `routes`: each row names two different experts; in each aligned block of 128 rows no expert is named more than 64 times, a bound that some block reaches. `log_decay`: negative at every position.
All inputs are finite; a program needn't handle non-finite values.
Results may differ from a plain program's by a relative error of at most 0.019.
Values may be sent and summed in bfloat16 or wider, within the bound.
No kernel may reach another device: no remote copies, remote signals or barrier semaphores. Data moves between devices by JAX's collectives and lax.ppermute only.
A program may use at most 64 MiB of HBM per device.

v0:
```python
import jax
import jax.numpy as jnp
from jax import lax
from jax.sharding import PartitionSpec as P

D = 4096
EPS = 1e-06
THETA = 10000.0


def entering_2(array, axis, combine, identity):
    devices, place = (lax.axis_size(axis), lax.axis_index(axis))
    everything = jax.tree.map(lambda part: lax.all_gather(part, axis), array)
    start = jax.tree.map(
        lambda part, zero: jnp.broadcast_to(jnp.asarray(zero, part.dtype), part.shape),
        array,
        identity,
    )

    def step(k, before):
        reached = k < place
        new = combine(before, jax.tree.map(lambda part: part[k], everything))
        return jax.tree.map(lambda a, b: jnp.where(reached, a, b), new, before)

    return lax.fori_loop(0, devices, step, start)


def rotate(block, positions):
    half_dim = block.shape[-1] // 2
    inverse = jnp.power(THETA, -jnp.arange(half_dim, dtype=jnp.float32) * 2.0 / block.shape[-1])
    angles = positions[:, None, None] * inverse
    cosine_val, sine_val = (jnp.cos(angles), jnp.sin(angles))
    lower_half, upper_half = (block[..., :half_dim], block[..., half_dim:])
    return jnp.concatenate(
        [
            lower_half * cosine_val - upper_half * sine_val,
            upper_half * cosine_val + lower_half * sine_val,
        ],
        axis=-1,
    )


def block_terms(rot_queries, rot_keys, value_heads, rates):
    count = rates.shape[0]
    decay_sum = jnp.cumsum(rates, axis=0)
    by_head = decay_sum.T
    causal = (jnp.arange(count)[:, None] >= jnp.arange(count)[None, :])[None]
    spread = by_head[:, :, None] - by_head[:, None, :]
    weight = jnp.where(causal, jnp.exp(jnp.where(causal, spread, 0.0)), 0.0)
    scores = jnp.einsum("ihd,jhd->hij", rot_queries, rot_keys, preferred_element_type=jnp.float32)
    weighted = (scores * weight).astype(jnp.bfloat16)
    within = jnp.einsum("hij,jhv->ihv", weighted, value_heads, preferred_element_type=jnp.float32)
    block_end = decay_sum[-1]
    carried = (
        rot_keys.astype(jnp.float32) * jnp.exp(block_end[None, :] - decay_sum)[:, :, None]
    ).astype(jnp.bfloat16)
    update = jnp.einsum("jhd,jhv->hdv", carried, value_heads, preferred_element_type=jnp.float32)
    return (within, decay_sum, jnp.exp(block_end), update)


def final_result(rot_queries, decay_sum, within, state_in, gate_part, gain_part):
    cross_part = (
        jnp.einsum(
            "ihd,hdv->ihv",
            rot_queries.astype(jnp.float32),
            state_in,
            precision=lax.Precision.HIGHEST,
        )
        * jnp.exp(decay_sum)[:, :, None]
    )
    retained = within + cross_part
    scaled = retained * lax.rsqrt(jnp.mean(retained * retained, axis=-1, keepdims=True) + EPS)
    count, head_count, value_size = retained.shape
    gated = jax.nn.silu(gate_part.astype(jnp.float32)).reshape(count, head_count, value_size)
    return (
        (scaled * gain_part.reshape(head_count, value_size) * gated)
        .reshape(count, -1)
        .astype(jnp.bfloat16)
    )


def prepare(queries, keys_in, value_part, positions, head_count):
    row_count = queries.shape[0]
    key_size = queries.shape[1] // head_count
    rot_queries = rotate(
        queries.astype(jnp.float32).reshape(row_count, head_count, key_size), positions
    ).astype(jnp.bfloat16)
    rot_keys = (
        rotate(keys_in.astype(jnp.float32).reshape(row_count, head_count, key_size), positions)
        * key_size ** (-0.5)
    ).astype(jnp.bfloat16)
    value_heads = value_part.reshape(row_count, head_count, value_part.shape[1] // head_count)
    return (rot_queries, rot_keys, value_heads)


def per_device(
    residual,
    query_small,
    key_narrow_group,
    query_large,
    key_large,
    values,
    gates,
    log_decay,
    head_gain,
    out_weight,
    norm_gain,
    routes,
    route_weight,
    expert_gate,
    expert_up,
    expert_down,
):
    row_count = residual.shape[0]
    head_count = log_decay.shape[2]
    positions = (lax.axis_index("sp") * row_count + jnp.arange(row_count, dtype=jnp.int32)).astype(
        jnp.float32
    )
    query_a, key_a, value_a = prepare(
        query_small, key_narrow_group, values[:, 0], positions, head_count
    )
    query_b, key_b, value_b = prepare(query_large, key_large, values[:, 1], positions, head_count)
    within_a, decay_sum_a, fall_a, update_a = block_terms(query_a, key_a, value_a, log_decay[:, 0])
    within_b, decay_sum_b, fall_b, update_b = block_terms(query_b, key_b, value_b, log_decay[:, 1])

    def combine(before_part, after_part):
        return (
            before_part[0] * after_part[0],
            after_part[0][:, None, None] * before_part[1] + after_part[1],
            before_part[2] * after_part[2],
            after_part[2][:, None, None] * before_part[3] + after_part[3],
        )

    identity = (
        jnp.ones_like(fall_a),
        jnp.zeros_like(update_a),
        jnp.ones_like(fall_b),
        jnp.zeros_like(update_b),
    )
    entering = entering_2((fall_a, update_a, fall_b, update_b), "sp", combine, identity)
    output_a = final_result(query_a, decay_sum_a, within_a, entering[1], gates[:, 0], head_gain[0])
    output_b = final_result(query_b, decay_sum_b, within_b, entering[3], gates[:, 1], head_gain[1])
    stacked = jnp.stack([output_a, output_b], axis=1)
    gathered = lax.all_gather(stacked, "tp", axis=2, tiled=True)
    mixed = jnp.einsum(
        "tgk,gkd->td",
        gathered,
        lax.all_gather(out_weight, "sp", axis=1, tiled=True),
        preferred_element_type=jnp.float32,
    ).astype(jnp.bfloat16)
    stream = residual.astype(jnp.float32) + mixed.astype(jnp.float32)
    square_sum = lax.psum(jnp.sum(stream * stream, axis=1), "tp")
    normed = (stream * lax.rsqrt(square_sum / D + EPS)[:, None] * norm_gain[None, :]).astype(
        jnp.bfloat16
    )
    experts = lax.axis_size("sp")
    capacity = 4 * row_count // experts
    one_hot = (routes[:, :, None] == jnp.arange(experts, dtype=jnp.int32)[None, None, :]).astype(
        jnp.int32
    )
    one_hot = one_hot.reshape(2 * row_count, experts)
    before = jnp.cumsum(one_hot, axis=0) - one_hot
    slot_index = jnp.sum(before * one_hot, axis=1).reshape(row_count, 2)
    target = routes * capacity + slot_index
    slot_ids = jnp.arange(experts * capacity, dtype=jnp.int32)
    choose = target[:, :, None] == slot_ids[None, None, :]
    select = jnp.sum(choose.astype(jnp.int32), axis=1).astype(jnp.bfloat16).T
    w_gate, w_up, w_down = (expert_gate[0], expert_up[0], expert_down[0])
    outgoing = jnp.dot(select, normed, preferred_element_type=jnp.float32).astype(jnp.bfloat16)
    outgoing = outgoing.reshape(experts, capacity, normed.shape[1])
    arrived = lax.all_to_all(outgoing, "sp", split_axis=0, concat_axis=0, tiled=True)
    expert_arrived = lax.all_gather(arrived, "tp", axis=2, tiled=True)
    gate_part = jnp.einsum(
        "sck,kf->scf", expert_arrived, w_gate, preferred_element_type=jnp.float32
    )
    up_part = jnp.einsum("sck,kf->scf", expert_arrived, w_up, preferred_element_type=jnp.float32)
    hidden = (jax.nn.silu(gate_part) * up_part).astype(jnp.bfloat16)
    expert_out = jnp.einsum(
        "scf,fd->scd",
        lax.all_gather(hidden, "tp", axis=2, tiled=True),
        w_down,
        preferred_element_type=jnp.float32,
    ).astype(jnp.bfloat16)
    returned = lax.all_to_all(expert_out, "sp", split_axis=0, concat_axis=0, tiled=True).reshape(
        experts * capacity, -1
    )
    first_pick = jnp.dot(
        choose[:, 0].astype(jnp.bfloat16), returned, preferred_element_type=jnp.float32
    )
    second_pick = jnp.dot(
        choose[:, 1].astype(jnp.bfloat16), returned, preferred_element_type=jnp.float32
    )
    routed = route_weight[:, 0:1] * first_pick + route_weight[:, 1:2] * second_pick
    return (stream + routed).astype(jnp.bfloat16)


def solution(mesh):
    placed = (
        P("sp", "tp"),
        P("sp", "tp"),
        P("sp", "tp"),
        P("sp", "tp"),
        P("sp", "tp"),
        P("sp", None, "tp"),
        P("sp", None, "tp"),
        P("sp", None, "tp"),
        P(None, "tp"),
        P(None, "sp", "tp"),
        P("tp"),
        P("sp", None),
        P("sp", None),
        P("sp", None, "tp"),
        P("sp", None, "tp"),
        P("sp", None, "tp"),
    )
    return jax.shard_map(
        per_device, mesh=mesh, in_specs=placed, out_specs=P("sp", "tp"), check_vma=False
    )
```

profile of v0, /device:TPU:0, one launch (start us, length us, event | category | flops | bytes accessed | tf_op | source)
XLA Modules:
  0.0 408.3 jit_solution(11339238263994428955)
XLA Ops:
  6.6 0.7 slice_bitcast_fusion.4
  7.3 1.5 fusion.79
  8.8 1.0 copy.129
  10.1 1.0 copy.132
  12.7 1.0 fusion.45
  15.9 1.2 fusion.32
  18.2 13.6 %all-gather.3 = f32[8,1,4]{2,1,0:T(1,128)S(1)} all-gather(f32[1,1,4]{2,1,0:T(1,128)S(1)} %get-tuple-element.253), channel_id=1, replica_groups=mesh['sp'=8,'tp'=4] {'sp'}, dimensions={0}, use_global_device_ids=true | all-gather | bytes 144 | tf_op jit(solution)/shard_map/all_gather | solution.py:13
  31.8 9.0 %all-gather.2 = f32[8,1,4]{2,1,0:T(1,128)S(1)} all-gather(f32[1,1,4]{2,1,0:T(1,128)S(1)} %get-tuple-element.255), channel_id=1, replica_groups=mesh['sp'=8,'tp'=4] {'sp'}, dimensions={0}, use_global_device_ids=true | all-gather | bytes 144 | tf_op jit(solution)/shard_map/all_gather | solution.py:13
  40.8 0.4 convolution_bitcast_fusion.4
  41.3 4.5 %all-gather.19.cloned.1.call-done = f32[32,128,128]{2,1,0:T(8,128)} async-done(((f32[4,128,128]{2,1,0:T(8,128)}), f32[32,128,128]{2,1,0:T(8,128)}) %all-gather.19.cloned.1.call-update) | async-done | bytes 2097168 | tf_op jit(solution)/shard_map/all_gather | solution.py:13
  45.8 47.9 %all-gather.21.cloned.1.call-done = f32[32,256,128]{2,1,0:T(8,128)} async-done(((f32[4,256,128]{2,1,0:T(8,128)}), f32[32,256,128]{2,1,0:T(8,128)}) %all-gather.21.cloned.1.call-update) | async-done | bytes 4194320 | tf_op jit(solution)/shard_map/all_gather | solution.py:13
  93.7 18.1 %while.16 = (s32[]{:T(128)}, f32[4,128,128]{2,1,0:T(8,128)S(1)}, f32[4,256,128]{2,1,0:T(8,128)S(1)}, s32[]{:T(128)}, f32[8,4]{1,0:T(8,128)S(1)}, /*index=5*/f32[...) while((s32[]{:T(128)}, f32[4,128,128]{2,1,0:T(8,128)S(1)}, ...), condition=%wide.region_3.4_spmd.clone, body=%wide.region_2.3_spmd.clone.sunk | while | flops 786436 | bytes 2359527 | solution.py:25
  93.7 1.2 fusion.106
  94.9 1.1 fusion.105
  96.0 1.2 fusion.106
  97.2 1.1 fusion.105
  98.2 1.2 fusion.106
  99.4 1.1 fusion.105
  100.5 1.2 fusion.106
  101.7 1.1 fusion.105
  102.8 1.2 fusion.106
  104.0 1.1 fusion.105
  105.1 1.2 fusion.106
  106.2 1.1 fusion.105
  107.3 1.2 fusion.106
  108.5 1.1 fusion.105
  109.6 1.2 fusion.106
  110.8 1.1 fusion.105
  111.9 0.5 multiply_reduce_fusion.2
  112.6 0.6 fusion.25
  113.3 0.4 multiply_reduce_fusion.1
  113.9 0.7 pad_maximum_fusion.1
  114.7 0.5 all-gather.13.cloned.1.call-update
  115.7 0.6 reduce-window.6
  117.0 23.0 %all-gather.11.cloned.1.call-done = bf16[128,2,2048]{2,0,1:T(8,128)(2,1)} async-done(((bf16[128,2,512]{2,0,1:T(8,128)(2,1)}), bf16[128,2,2048]{2,0,1:T(8,128)(2,1)}) %all-gather.11.cloned.1.call-update) | async-done | bytes 1048592 | tf_op jit(solution)/shard_map/all_gather | solution.py:144
  140.0 83.5 %all-gather.13.cloned.1.call-done = bf16[2,2048,1024]{2,1,0:T(8,128)(2,1)} async-done(((bf16[2,256,1024]{2,1,0:T(8,128)(2,1)}), bf16[2,2048,1024]{2,1,0:T(8,128)(2,1)}) %all-gather.13.cloned.1.call-update) | async-done | bytes 8388624 | tf_op jit(solution)/shard_map/all_gather | solution.py:148
  223.6 5.1 %multiply_reduce_fusion = (f32[128]{0:T(128)S(1)}, f32[128,1024]{1,0:T(8,128)S(1)}) fusion(bf16[128,2,2048]{2,0,1:T(8,128)(2,1)} %all-gather.11.cloned.1.call-done, bf16[2,2048,1024]{2,1,0:T(8,128)(2,1)} %all-gather.13.cloned.1.call-done, bf16[128,1024]{1,0:T(8,128)(2,1)S(1)} %copy-done.1), kind=kOutput, calls=%fused_computation.42 | convolution fusion | flops 1074528128 | bytes 10224128 | tf_op jit(solution)/shard_map/tgk,gkd->td/dot_general | solution.py:145
  228.6 9.8 %psum.7 = f32[128]{0:T(128)S(1)} all-reduce(f32[128]{0:T(128)S(1)} %get-tuple-element.270), channel_id=1, replica_groups=mesh['sp'=8,'tp'=4] {'tp'}, use_global_device_ids=true, to_apply=%region_11.12 | all-reduce | flops 128 | bytes 1024 | tf_op jit(solution)/shard_map/psum | solution.py:152
  238.5 0.5 convolution_convert_fusion
  239.0 29.7 %all_to_all.10 = bf16[8,64,1024]{2,1,0:T(8,128)(2,1)} all-to-all(bf16[8,64,1024]{2,1,0:T(8,128)(2,1)S(1)} %bitcast.130), channel_id=1, replica_groups=mesh['sp'=8,'tp'=4] {'sp'}, dimensions={0} | all-to-all | bytes 2097152 | tf_op jit(solution)/shard_map/all_to_all | solution.py:171
  268.9 49.5 %all-gather.15.cloned.1.call-done = bf16[8,64,4096]{2,1,0:T(8,128)(2,1)} async-done(((bf16[8,64,1024]{2,1,0:T(8,128)(2,1)}), bf16[8,64,4096]{2,1,0:T(8,128)(2,1)}) %all-gather.15.cloned.1.call-update) | async-done | bytes 4194320 | tf_op jit(solution)/shard_map/all_gather | solution.py:172
  318.5 5.9 %fusion.8 = f32[8,64,512]{2,1,0:T(8,128)S(1)} fusion(bf16[8,64,4096]{2,1,0:T(8,128)(2,1)} %all-gather.15.cloned.1.call-done, bf16[1,4096,512]{2,1,0:T(8,128)(2,1)} %param.31), kind=kOutput, calls=%fused_computation.12 | convolution fusion | flops 2147483648 | bytes 9437184 | tf_op jit(solution)/shard_map/sck,kf->scf/dot_general | solution.py:173
  324.4 3.2 fusion.16
  327.7 35.2 %all-gather.17.cloned.1.call-done = bf16[8,64,2048]{2,1,0:T(8,128)(2,1)} async-done(((bf16[8,64,512]{2,1,0:T(8,128)(2,1)}), bf16[8,64,2048]{2,1,0:T(8,128)(2,1)}) %all-gather.17.cloned.1.call-update) | async-done | bytes 2097168 | tf_op jit(solution)/shard_map/all_gather | solution.py:180
  362.8 6.1 %fusion.10 = bf16[8,64,1024]{2,1,0:T(8,128)(2,1)} fusion(bf16[8,64,2048]{2,1,0:T(8,128)(2,1)} %all-gather.17.cloned.1.call-done, bf16[1,2048,1024]{2,1,0:T(8,128)(2,1)} %param.33), kind=kOutput, calls=%fused_computation.15 | convolution fusion | flops 2148007936 | bytes 7340032 | tf_op jit(solution)/shard_map/scf,fd->scd/dot_general | solution.py:178
  369.0 4.6 %all-to-all-start.1 = ((bf16[8,64,1024]{2,1,0:T(8,128)(2,1)}), bf16[8,64,1024]{2,1,0:T(8,128)(2,1)S(1)}, u32[]{:S(2)}, u32[]{:S(2)}) async-start(bf16[8,64,1024]{2,1,0:T(8,128)(2,1)} %fusion.10), calls=%async_computation.1 | async-start | bytes 2097152 | tf_op jit(solution)/shard_map/all_to_all | solution.py:184
  373.7 26.4 %all-to-all-done.1 = bf16[8,64,1024]{2,1,0:T(8,128)(2,1)S(1)} async-done(((bf16[8,64,1024]{2,1,0:T(8,128)(2,1)}), bf16[8,64,1024]{2,1,0:T(8,128)(2,1)S(1)}, u32[]{:S(2)}, u32[]{:S(2)}) %all-to-all-start.1) | async-done | bytes 1048608 | tf_op jit(solution)/shard_map/all_to_all | solution.py:184
  400.5 1.0 fusion.24
  (107 shorter events, 7.4 us)
Async XLA Ops:
  6.5 39.3 %all-gather.19.cloned.1.call-start = ((), (), s32[]{:S(2)}) async-start(), calls=%async_computation.6 | async-start | bytes 2359296 | tf_op jit(solution)/shard_map/all_gather | solution.py:13
  7.3 6.5 %copy-start.2 = (bf16[128,1024]{1,0:T(8,128)(2,1)S(1)}, bf16[128,1024]{1,0:T(8,128)(2,1)}, u32[]{:S(2)}) copy-start(bf16[128,1024]{1,0:T(8,128)(2,1)} %param.22) | copy-start | bytes 786436
  11.2 3.1 copy-start.3
  13.7 80.0 %all-gather.21.cloned.1.call-start = ((), (), s32[]{:S(2)}) async-start(), calls=%async_computation.7 | async-start | bytes 4718592 | tf_op jit(solution)/shard_map/all_gather | solution.py:13
  14.0 3.3 copy-start
  14.8 26.0 %copy-start.6 = (f32[2,512]{1,0:T(2,128)S(1)}, f32[2,512]{1,0:T(2,128)}, u32[]{:S(2)}) copy-start(f32[2,512]{1,0:T(2,128)} %param.26) | copy-start | bytes 12292
  17.1 122.9 %all-gather.11.cloned.1.call-start = ((), (), s32[]{:S(2)}) async-start(), calls=%async_computation.2 | async-start | bytes 1310720 | tf_op jit(solution)/shard_map/all_gather | solution.py:144
  111.8 3.5 copy-start.5
  111.9 111.7 %copy-start.1 = (bf16[128,1024]{1,0:T(8,128)(2,1)S(1)}, bf16[128,1024]{1,0:T(8,128)(2,1)}, u32[]{:S(2)}) copy-start(bf16[128,1024]{1,0:T(8,128)(2,1)} %param.18) | copy-start | bytes 786436
  114.7 108.9 %all-gather.13.cloned.1.call-start = ((), (), s32[]{:S(2)}) async-start(), calls=%async_computation.3 | async-start | bytes 9437184 | tf_op jit(solution)/shard_map/all_gather | solution.py:148
  115.3 203.2 %all-gather.15.cloned.1.call-start = ((), (), s32[]{:S(2)}) async-start(), calls=%async_computation.4 | async-start | bytes 5242880 | tf_op jit(solution)/shard_map/all_gather | solution.py:172
  117.0 121.4 %copy-start.4 = (f32[1024]{0:T(1024)S(1)}, f32[1024]{0:T(1024)}, u32[]{:S(2)}) copy-start(f32[1024]{0:T(1024)} %param.28) | copy-start | bytes 12292
  268.7 94.2 %all-gather.17.cloned.1.call-start = ((), (), s32[]{:S(2)}) async-start(), calls=%async_computation.5 | async-start | bytes 2621440 | tf_op jit(solution)/shard_map/all_gather | solution.py:180
  318.5 5.9 %copy-start.8 = (bf16[1,4096,512]{2,1,0:T(8,128)(2,1)S(1)}, bf16[1,4096,512]{2,1,0:T(8,128)(2,1)}, u32[]{:S(2)}) copy-start(bf16[1,4096,512]{2,1,0:T(8,128)(2,1)} %param.32) | copy-start | bytes 12582916
  318.5 5.9 %copy-start.9 = (bf16[8,64,4096]{2,1,0:T(8,128)(2,1)S(1)}, bf16[8,64,4096]{2,1,0:T(8,128)(2,1)}, u32[]{:S(2)}) copy-start(bf16[8,64,4096]{2,1,0:T(8,128)(2,1)} %all-gather.15.cloned.1.call-done) | copy-start | bytes 12582916
  327.6 45.9 %copy-start.7 = (f32[128,2]{0,1:T(2,128)S(1)}, f32[128,2]{0,1:T(2,128)}, u32[]{:S(2)}) copy-start(f32[128,2]{0,1:T(2,128)} %param.30) | copy-start | bytes 3076
  369.0 31.2 %all-to-all-start.1 = ((bf16[8,64,1024]{2,1,0:T(8,128)(2,1)}), bf16[8,64,1024]{2,1,0:T(8,128)(2,1)S(1)}, u32[]{:S(2)}, u32[]{:S(2)}) async-start(bf16[8,64,1024]{2,1,0:T(8,128)(2,1)} %fusion.10), calls=%async_computation.1 | async-start | bytes 2097152 | tf_op jit(solution)/shard_map/all_to_all | solution.py:184
Sparse Core Ops, SparseCore 0:
  13.9 31.9 all-gather.18
  47.4 46.2 all-gather.20
  114.8 25.1 all-gather.10
  141.5 82.0 all-gather.12
  268.8 49.6 all-gather.14
  327.8 35.0 all-gather.16
where the time goes:
time: 409 us; the launch traced here: 408 us
  waiting for transfers between devices  271 us (66%)
  blocking collectives  62.1 us (15%)
  matrix products  26.3 us (6%)
  other arithmetic  21.3 us (5%)
  between operations  14 us (3%)
  local copies, waits for them, and re-layouts  8.67 us (2%)
  starting transfers between devices  4.99 us (1%)
    all_gather x1, waiting for transfers between devices, per_device(): lax.all_gather(out_weight, 'sp', axis=1, tiled=True)  83.5 us
    all_gather x2, waiting for transfers between devices, entering_2(): everything = jax.tree.map(lambda part: lax.all_gather(part, axis), array)  52.4 us
    all_gather x1, waiting for transfers between devices, per_device(): expert_arrived = lax.all_gather(arrived, 'tp', axis=2, tiled=True)  49.5 us
    all_gather x1, waiting for transfers between devices, per_device(): lax.all_gather(hidden, 'tp', axis=2, tiled=True)  35.2 us
    all_to_all x1, blocking collectives, per_device(): lax.all_to_all(outgoing, 'sp', split_axis=0, concat_axis=0, tiled=True)  29.7 us
    all_to_all x1, waiting for transfers between devices, per_device(): lax.all_to_all(expert_out, 'sp', split_axis=0, concat_axis=0, tiled=True)  26.4 us
    all_gather x1, waiting for transfers between devices, per_device(): gathered = lax.all_gather(stacked, 'tp', axis=2, tiled=True)  23 us
    all_gather x2, blocking collectives, entering_2(): everything = jax.tree.map(lambda part: lax.all_gather(part, axis), array)  22.6 us
  transfers between devices with their start and end apart: 7, of which 7 were waited for; matrix products, arithmetic and copies ran while one was open for 2% of the time, Pallas kernels for 0%

commit v1 on v0

--- a/solution.py
+++ b/solution.py
@@ -169,7 +169,12 @@
     outgoing = jnp.dot(select, normed, preferred_element_type=jnp.float32).astype(jnp.bfloat16)
     outgoing = outgoing.reshape(experts, capacity, normed.shape[1])
     arrived = lax.all_to_all(outgoing, "sp", split_axis=0, concat_axis=0, tiled=True)
-    expert_arrived = lax.all_gather(arrived, "tp", axis=2, tiled=True)
+    ring = [arrived]
+    for hop in range(3):
+        ring.append(lax.ppermute(ring[-1], "tp", [(dev, (dev + 1) % 4) for dev in range(4)]))
+    expert_arrived = jnp.roll(
+        jnp.concatenate(ring[::-1], axis=2), (lax.axis_index("tp") + 1) * ring[0].shape[2], axis=2
+    )
     gate_part = jnp.einsum(
         "sck,kf->scf", expert_arrived, w_gate, preferred_element_type=jnp.float32
     )

time: 409 us -> 434 us (1.061)
  waiting for transfers between devices: 271 us -> 294 us
  local copies, waits for them, and re-layouts: 8.67 us -> 14.3 us
    ppermute x0 -> x3, waiting for transfers between devices: none -> 74.1 us  [per_device(): lax.ppermute(ring[-1], 'tp', [(dev, (dev + 1) % 4) for dev in range(4)])]
    all_gather x1 -> x0, waiting for transfers between devices: 49.5 us -> none  [per_device(): expert_arrived = lax.all_gather(arrived, 'tp', axis=2, tiled=True)]
    unnamed x34 -> x41, local copies, waits for them, and re-layouts: 3.78 us -> 9.27 us
  transfers between devices with their start and end apart: 7 -> 9, of which waited for: 7 -> 9; matrix products, arithmetic and copies ran while one was open for 2% -> 1% of each run, Pallas kernels for 0% -> 0%
where the time goes in v1:
time: 434 us; the launch traced here: 433 us
  waiting for transfers between devices  294 us (68%)
  blocking collectives  61.4 us (14%)
  matrix products  22.7 us (5%)
  other arithmetic  21.4 us (5%)
  local copies, waits for them, and re-layouts  14.3 us (3%)
  between operations  13.7 us (3%)
  starting transfers between devices  4.78 us (1%)
    all_gather x1, waiting for transfers between devices, per_device(): lax.all_gather(out_weight, 'sp', axis=1, tiled=True)  83.5 us
    ppermute x3, waiting for transfers between devices, per_device(): lax.ppermute(ring[-1], 'tp', [(dev, (dev + 1) % 4) for dev in range(4)])  74.1 us
    all_gather x2, waiting for transfers between devices, entering_2(): everything = jax.tree.map(lambda part: lax.all_gather(part, axis), array)  52.5 us
    all_gather x1, waiting for transfers between devices, per_device(): lax.all_gather(hidden, 'tp', axis=2, tiled=True)  34 us
    all_to_all x1, blocking collectives, per_device(): lax.all_to_all(outgoing, 'sp', split_axis=0, concat_axis=0, tiled=True)  29 us
    all_to_all x1, waiting for transfers between devices, per_device(): lax.all_to_all(expert_out, 'sp', split_axis=0, concat_axis=0, tiled=True)  26.4 us
    all_gather x1, waiting for transfers between devices, per_device(): gathered = lax.all_gather(stacked, 'tp', axis=2, tiled=True)  23 us
    all_gather x2, blocking collectives, entering_2(): everything = jax.tree.map(lambda part: lax.all_gather(part, axis), array)  22.6 us
  transfers between devices with their start and end apart: 9, of which 9 were waited for; matrix products, arithmetic and copies ran while one was open for 1% of the time, Pallas kernels for 0%

profile of v1, /device:TPU:0, one launch (start us, length us, event | category | flops | bytes accessed | tf_op | source)
XLA Modules:
  0.0 432.8 jit_solution(8261201068690864500)
XLA Ops:
  6.6 0.8 slice_bitcast_fusion.4
  7.3 1.5 fusion.81
  8.9 1.0 copy.129
  10.2 1.0 copy.132
  12.8 1.0 fusion.41
  15.9 1.2 fusion.28
  18.2 13.6 %all-gather.3 = f32[8,1,4]{2,1,0:T(1,128)S(1)} all-gather(f32[1,1,4]{2,1,0:T(1,128)S(1)} %get-tuple-element.253), channel_id=1, replica_groups=mesh['sp'=8,'tp'=4] {'sp'}, dimensions={0}, use_global_device_ids=true | all-gather | bytes 144 | tf_op jit(solution)/shard_map/all_gather | solution.py:13
  31.8 9.0 %all-gather.2 = f32[8,1,4]{2,1,0:T(1,128)S(1)} all-gather(f32[1,1,4]{2,1,0:T(1,128)S(1)} %get-tuple-element.255), channel_id=1, replica_groups=mesh['sp'=8,'tp'=4] {'sp'}, dimensions={0}, use_global_device_ids=true | all-gather | bytes 144 | tf_op jit(solution)/shard_map/all_gather | solution.py:13
  41.3 4.6 %all-gather.16.cloned.1.call-done = f32[32,128,128]{2,1,0:T(8,128)} async-done(((f32[4,128,128]{2,1,0:T(8,128)}), f32[32,128,128]{2,1,0:T(8,128)}) %all-gather.16.cloned.1.call-update) | async-done | bytes 2097168 | tf_op jit(solution)/shard_map/all_gather | solution.py:13
  45.9 47.9 %all-gather.18.cloned.1.call-done = f32[32,256,128]{2,1,0:T(8,128)} async-done(((f32[4,256,128]{2,1,0:T(8,128)}), f32[32,256,128]{2,1,0:T(8,128)}) %all-gather.18.cloned.1.call-update) | async-done | bytes 4194320 | tf_op jit(solution)/shard_map/all_gather | solution.py:13
  93.8 18.2 %while.16 = (s32[]{:T(128)}, f32[4,128,128]{2,1,0:T(8,128)S(1)}, f32[4,256,128]{2,1,0:T(8,128)S(1)}, s32[]{:T(128)}, f32[8,4]{1,0:T(8,128)S(1)}, /*index=5*/f32[...) while((s32[]{:T(128)}, f32[4,128,128]{2,1,0:T(8,128)S(1)}, ...), condition=%wide.region_3.4_spmd.clone, body=%wide.region_2.3_spmd.clone.sunk | while | flops 786436 | bytes 2359527 | solution.py:25
  93.8 1.2 fusion.106
  95.0 1.1 fusion.105
  96.1 1.2 fusion.106
  97.3 1.1 fusion.105
  98.4 1.2 fusion.106
  99.6 1.1 fusion.105
  100.7 1.2 fusion.106
  101.8 1.1 fusion.105
  102.9 1.2 fusion.106
  104.1 1.1 fusion.105
  105.2 1.2 fusion.106
  106.4 1.1 fusion.105
  107.5 1.2 fusion.106
  108.7 1.1 fusion.105
  109.8 1.2 fusion.106
  110.9 1.1 fusion.105
  112.8 0.7 fusion.21
  114.1 0.7 pad_maximum_fusion.1
  117.2 23.0 %all-gather.10.cloned.1.call-done = bf16[128,2,2048]{2,0,1:T(8,128)(2,1)} async-done(((bf16[128,2,512]{2,0,1:T(8,128)(2,1)}), bf16[128,2,2048]{2,0,1:T(8,128)(2,1)}) %all-gather.10.cloned.1.call-update) | async-done | bytes 1048592 | tf_op jit(solution)/shard_map/all_gather | solution.py:144
  140.2 83.5 %all-gather.12.cloned.1.call-done = bf16[2,2048,1024]{2,1,0:T(8,128)(2,1)} async-done(((bf16[2,256,1024]{2,1,0:T(8,128)(2,1)}), bf16[2,2048,1024]{2,1,0:T(8,128)(2,1)}) %all-gather.12.cloned.1.call-update) | async-done | bytes 8388624 | tf_op jit(solution)/shard_map/all_gather | solution.py:148
  223.7 5.1 %multiply_reduce_fusion = (f32[128]{0:T(128)S(1)}, f32[128,1024]{1,0:T(8,128)S(1)}) fusion(bf16[128,2,2048]{2,0,1:T(8,128)(2,1)} %all-gather.10.cloned.1.call-done, bf16[2,2048,1024]{2,1,0:T(8,128)(2,1)} %all-gather.12.cloned.1.call-done, bf16[128,1024]{1,0:T(8,128)(2,1)S(1)} %copy-done.1), kind=kOutput, calls=%fused_computation.43 | convolution fusion | flops 1074528128 | bytes 10224128 | tf_op jit(solution)/shard_map/tgk,gkd->td/dot_general | solution.py:145
  228.8 9.8 %psum.7 = f32[128]{0:T(128)S(1)} all-reduce(f32[128]{0:T(128)S(1)} %get-tuple-element.270), channel_id=1, replica_groups=mesh['sp'=8,'tp'=4] {'tp'}, use_global_device_ids=true, to_apply=%region_11.12 | all-reduce | flops 128 | bytes 1024 | tf_op jit(solution)/shard_map/psum | solution.py:152
  239.2 29.0 %all_to_all.10 = bf16[8,64,1024]{2,1,0:T(8,128)(2,1)S(1)} all-to-all(bf16[8,64,1024]{2,1,0:T(8,128)(2,1)S(1)} %bitcast.126), channel_id=1, replica_groups=mesh['sp'=8,'tp'=4] {'sp'}, dimensions={0} | all-to-all | bytes 2097152 | tf_op jit(solution)/shard_map/all_to_all | solution.py:171
  268.1 25.4 %collective-permute-done = bf16[8,64,1024]{2,1,0:T(8,128)(2,1)S(1)} collective-permute-done((bf16[8,64,1024]{2,1,0:T(8,128)(2,1)S(1)}, bf16[8,64,1024]{2,1,0:T(8,128)(2,1)S(1)}, u32[]{:S(2)}, u32[]{:S(2)}) %collective-permute-start) | collective-permute-done | bytes 1048608 | tf_op jit(solution)/shard_map/ppermute | solution.py:174
  293.6 24.7 %collective-permute-done.1 = bf16[8,64,1024]{2,1,0:T(8,128)(2,1)} collective-permute-done((bf16[8,64,1024]{2,1,0:T(8,128)(2,1)S(1)}, bf16[8,64,1024]{2,1,0:T(8,128)(2,1)}, u32[]{:S(2)}, u32[]{:S(2)}) %collective-permute-start.1) | collective-permute-done | bytes 1048608 | tf_op jit(solution)/shard_map/ppermute | solution.py:174
  318.3 24.0 %collective-permute-done.2 = bf16[8,64,1024]{2,1,0:T(8,128)(2,1)} collective-permute-done((bf16[8,64,1024]{2,1,0:T(8,128)(2,1)}, bf16[8,64,1024]{2,1,0:T(8,128)(2,1)}, u32[]{:S(2)}, u32[]{:S(2)}) %collective-permute-start.2) | collective-permute-done | bytes 1048608 | tf_op jit(solution)/shard_map/ppermute | solution.py:174
  342.3 1.3 constant_dynamic-update-slice_fusion.7
  343.6 1.3 constant_dynamic-update-slice_fusion.6
  345.1 1.3 constant_dynamic-update-slice_fusion.3
  346.4 1.3 constant_dynamic-update-slice_fusion.2
  348.0 2.3 fusion.8
  350.3 3.2 multiply_convert_fusion
  353.5 34.0 %all-gather.14.cloned.1.call-done = bf16[8,64,2048]{2,1,0:T(8,128)(2,1)} async-done(((bf16[8,64,512]{2,1,0:T(8,128)(2,1)}), bf16[8,64,2048]{2,1,0:T(8,128)(2,1)}) %all-gather.14.cloned.1.call-update) | async-done | bytes 2097168 | tf_op jit(solution)/shard_map/all_gather | solution.py:185
  387.6 6.1 %fusion.12 = bf16[8,64,1024]{2,1,0:T(8,128)(2,1)} fusion(bf16[8,64,2048]{2,1,0:T(8,128)(2,1)} %all-gather.14.cloned.1.call-done, bf16[1,2048,1024]{2,1,0:T(8,128)(2,1)} %param.33), kind=kOutput, calls=%fused_computation.17 | convolution fusion | flops 2148007936 | bytes 7340032 | tf_op jit(solution)/shard_map/scf,fd->scd/dot_general | solution.py:183
  393.7 4.6 %all-to-all-start.1 = ((bf16[8,64,1024]{2,1,0:T(8,128)(2,1)}), bf16[8,64,1024]{2,1,0:T(8,128)(2,1)S(1)}, u32[]{:S(2)}, u32[]{:S(2)}) async-start(bf16[8,64,1024]{2,1,0:T(8,128)(2,1)} %fusion.12), calls=%async_computation.1 | async-start | bytes 2097152 | tf_op jit(solution)/shard_map/all_to_all | solution.py:189
  398.5 26.4 %all-to-all-done.1 = bf16[8,64,1024]{2,1,0:T(8,128)(2,1)S(1)} async-done(((bf16[8,64,1024]{2,1,0:T(8,128)(2,1)}), bf16[8,64,1024]{2,1,0:T(8,128)(2,1)S(1)}, u32[]{:S(2)}, u32[]{:S(2)}) %all-to-all-start.1) | async-done | bytes 1048608 | tf_op jit(solution)/shard_map/all_to_all | solution.py:189
  425.2 1.0 fusion.20
  (118 shorter events, 10.4 us)
Async XLA Ops:
  6.5 7.3 %copy-start.2 = (bf16[128,1024]{1,0:T(8,128)(2,1)S(1)}, bf16[128,1024]{1,0:T(8,128)(2,1)}, u32[]{:S(2)}) copy-start(bf16[128,1024]{1,0:T(8,128)(2,1)} %param.22) | copy-start | bytes 786436
  6.5 7.8 %copy-start.3 = (bf16[128,1024]{1,0:T(8,128)(2,1)S(1)}, bf16[128,1024]{1,0:T(8,128)(2,1)}, u32[]{:S(2)}) copy-start(bf16[128,1024]{1,0:T(8,128)(2,1)} %param.21) | copy-start | bytes 786436
  6.5 39.4 %all-gather.16.cloned.1.call-start = ((), (), s32[]{:S(2)}) async-start(), calls=%async_computation.5 | async-start | bytes 2359296 | tf_op jit(solution)/shard_map/all_gather | solution.py:13
  9.9 7.4 %copy-start = (bf16[128,2,512]{2,1,0:T(2,128)(2,1)S(1)}, bf16[128,2,512]{2,1,0:T(2,128)(2,1)}, u32[]{:S(2)}) copy-start(bf16[128,2,512]{2,1,0:T(2,128)(2,1)} %param.24) | copy-start | bytes 786436
  12.5 28.4 %copy-start.6 = (f32[2,512]{1,0:T(2,128)S(1)}, f32[2,512]{1,0:T(2,128)}, u32[]{:S(2)}) copy-start(f32[2,512]{1,0:T(2,128)} %param.26) | copy-start | bytes 12292
  13.8 80.0 %all-gather.18.cloned.1.call-start = ((), (), s32[]{:S(2)}) async-start(), calls=%async_computation.6 | async-start | bytes 4718592 | tf_op jit(solution)/shard_map/all_gather | solution.py:13
  17.2 123.0 %all-gather.10.cloned.1.call-start = ((), (), s32[]{:S(2)}) async-start(), calls=%async_computation.2 | async-start | bytes 1310720 | tf_op jit(solution)/shard_map/all_gather | solution.py:144
  93.8 21.7 %copy-start.5 = (s32[128,2]{0,1:T(2,128)S(1)}, s32[128,2]{0,1:T(2,128)}, u32[]{:S(2)}) copy-start(s32[128,2]{0,1:T(2,128)} %param.29) | copy-start | bytes 3076
  93.8 129.9 %copy-start.1 = (bf16[128,1024]{1,0:T(8,128)(2,1)S(1)}, bf16[128,1024]{1,0:T(8,128)(2,1)}, u32[]{:S(2)}) copy-start(bf16[128,1024]{1,0:T(8,128)(2,1)} %param.18) | copy-start | bytes 786436
  114.8 108.9 %all-gather.12.cloned.1.call-start = ((), (), s32[]{:S(2)}) async-start(), calls=%async_computation.3 | async-start | bytes 9437184 | tf_op jit(solution)/shard_map/all_gather | solution.py:148
  115.4 123.2 %copy-start.4 = (f32[1024]{0:T(1024)S(1)}, f32[1024]{0:T(1024)}, u32[]{:S(2)}) copy-start(f32[1024]{0:T(1024)} %param.28) | copy-start | bytes 12292
  115.4 272.1 %all-gather.14.cloned.1.call-start = ((), (), s32[]{:S(2)}) async-start(), calls=%async_computation.4 | async-start | bytes 2621440 | tf_op jit(solution)/shard_map/all_gather | solution.py:185
  268.1 25.4 %collective-permute-start = (bf16[8,64,1024]{2,1,0:T(8,128)(2,1)S(1)}, bf16[8,64,1024]{2,1,0:T(8,128)(2,1)S(1)}, u32[]{:S(2)}, u32[]{:S(2)}) collective-permute-start(bf16[8,64,1024]{2,1,0:T(8,128)(2,1)S(1)} %all_to_all.10), channel_id=1, source_target_pairs={{0,1},{1,2},{2,3},{3,0},{4,5},{5,6},{6,7},{7,4},{8,9},{9,10},{10,1... | collective-permute-start | bytes 3145736 | tf_op jit(solution)/shard_map/ppermute | solution.py:174
  293.6 24.7 %collective-permute-start.1 = (bf16[8,64,1024]{2,1,0:T(8,128)(2,1)S(1)}, bf16[8,64,1024]{2,1,0:T(8,128)(2,1)}, u32[]{:S(2)}, u32[]{:S(2)}) collective-permute-start(bf16[8,64,1024]{2,1,0:T(8,128)(2,1)S(1)} %collective-permute-done), channel_id=1, source_target_pairs={{0,1},{1,2},{2,3},{3,0},{4,5},{5,6},{6,7},{7,4},{8,9},{9,10},{10,1... | collective-permute-start | bytes 3145736 | tf_op jit(solution)/shard_map/ppermute | solution.py:174
  318.3 24.0 %collective-permute-start.2 = (bf16[8,64,1024]{2,1,0:T(8,128)(2,1)}, bf16[8,64,1024]{2,1,0:T(8,128)(2,1)}, u32[]{:S(2)}, u32[]{:S(2)}) collective-permute-start(bf16[8,64,1024]{2,1,0:T(8,128)(2,1)} %collective-permute-done.1), channel_id=1, source_target_pairs={{0,1},{1,2},{2,3},{3,0},{4,5},{5,6},{6,7},{7,4},{8,9},{9,10},{10,1... | collective-permute-start | bytes 3145736 | tf_op jit(solution)/shard_map/ppermute | solution.py:174
  318.3 29.7 %copy-start.8 = (bf16[1,4096,512]{2,1,0:T(8,128)(2,1)S(1)}, bf16[1,4096,512]{2,1,0:T(8,128)(2,1)}, u32[]{:S(2)}) copy-start(bf16[1,4096,512]{2,1,0:T(8,128)(2,1)} %param.31) | copy-start | bytes 12582916
  348.0 2.3 copy-start.9
  353.5 44.8 %copy-start.7 = (f32[128,2]{0,1:T(2,128)S(1)}, f32[128,2]{0,1:T(2,128)}, u32[]{:S(2)}) copy-start(f32[128,2]{0,1:T(2,128)} %param.30) | copy-start | bytes 3076
  393.7 31.2 %all-to-all-start.1 = ((bf16[8,64,1024]{2,1,0:T(8,128)(2,1)}), bf16[8,64,1024]{2,1,0:T(8,128)(2,1)S(1)}, u32[]{:S(2)}, u32[]{:S(2)}) async-start(bf16[8,64,1024]{2,1,0:T(8,128)(2,1)} %fusion.12), calls=%async_computation.1 | async-start | bytes 2097152 | tf_op jit(solution)/shard_map/all_to_all | solution.py:189
Sparse Core Ops, SparseCore 0:
  13.9 31.9 all-gather.15
  47.5 46.2 all-gather.17
  115.0 25.1 all-gather.9
  141.7 82.0 all-gather.11
  353.7 33.8 all-gather.13
